TPU v7x, 32 devices: a whole 2x2x4 slice. The times are simulated.
32 devices in a mesh: ep: 8 (over z, core), tp: 4 (over y, x).
Axes of the slice: x: 2, y: 2, z: 4, core: 2. Of those that a mesh axis runs over, the one named last changes fastest.
Arguments:
- tokens: bfloat16 [256, 4096], P('ep', 'tp'), may hold values from -256 to 256
- expert_ids: int32 [256, 8], P('ep'), may hold values from 0 to 15, all different within a row; in each aligned block of 32 rows (0 to 31, 32 to 63, ...) at most 32 rows name the same one
- route_weights: float32 [256, 8], P('ep'), may hold values from 0.05 to 1
- gain_in: float32 [4096], P('tp'), may hold values from 0.1 to 1.9
- gain_out: float32 [4096], P('tp'), may hold values from 0.1 to 1.9
- gate_weights: bfloat16 [16, 4096, 1024], P('ep', 'tp'), may hold values from -0.09375 to 0.09375
- up_weights: bfloat16 [16, 4096, 1024], P('ep', 'tp'), may hold values from -0.09375 to 0.09375
- down_weights: bfloat16 [16, 1024, 4096], P('ep', None, 'tp'), may hold values from -0.1875 to 0.1875
Outputs:
- mixed: bfloat16 [256, 4096], P('ep', 'tp')
Inputs may be any that keep to these rules, and one draw needn't show every extreme that they name: `expert_ids`: each row names 8 different experts. Within the rows of one index of ep (aligned blocks of 32 rows) no expert is named more than 32 times, and in some blocks some expert is named exactly 32 times.
All inputs are finite; a program needn't handle non-finite values.
Results may differ from a plain program's by a relative error of at most 0.023.
Values may be sent and summed in bfloat16 or wider, within the bound.
A program may use at most 64 MiB of HBM per device.

v0:
```python
import jax
import jax.numpy as jnp
from jax import lax
from jax.sharding import PartitionSpec as P

D = 4096


epsilon = 1e-06


def expert_apply(incoming, gate_weights, up_weights, down_weights):
    gate_part = jnp.einsum(
        "secd,edf->secf", incoming, gate_weights, preferred_element_type=jnp.float32
    ).astype(jnp.bfloat16)
    up_part = jnp.einsum(
        "secd,edf->secf", incoming, up_weights, preferred_element_type=jnp.float32
    ).astype(jnp.bfloat16)
    gate_sum, up_sum = (
        lax.psum(gate_part, "tp").astype(jnp.float32),
        lax.psum(up_part, "tp").astype(jnp.float32),
    )
    hidden = (jax.nn.silu(gate_sum) * up_sum).astype(jnp.bfloat16)
    total = jnp.einsum("secf,efd->secd", hidden, down_weights, preferred_element_type=jnp.float32)
    return total.astype(jnp.bfloat16)


def on_device(
    tokens, expert_ids, route_weights, gain_in, gain_out, gate_weights, up_weights, down_weights
):
    tok_count, local_width = tokens.shape
    top_count = expert_ids.shape[1]
    local_experts = gate_weights.shape[0]
    ep_count = lax.axis_size("ep")
    all_experts = local_experts * ep_count
    capacity = max(2, 2 * tok_count * top_count // all_experts)
    widened = tokens.astype(jnp.float32)
    squares = lax.psum(jnp.sum(widened * widened, axis=1), "tp")
    normed = (widened * lax.rsqrt(squares / D + epsilon)[:, None] * gain_in[None, :]).astype(
        jnp.bfloat16
    )
    pair_ids = expert_ids.reshape(-1)
    expert_hot = (pair_ids[:, None] == jnp.arange(all_experts, dtype=jnp.int32)[None, :]).astype(
        jnp.int32
    )
    slot_rank = jnp.sum((jnp.cumsum(expert_hot, axis=0) - 1) * expert_hot, axis=1)
    slot_ids = pair_ids * capacity + slot_rank
    slot_hot = (
        slot_ids[:, None] == jnp.arange(all_experts * capacity, dtype=jnp.int32)[None, :]
    ).astype(jnp.float32)
    pair_rows = jnp.repeat(normed, top_count, axis=0)
    outgoing = jnp.einsum(
        "ps,pd->sd", slot_hot.astype(jnp.bfloat16), pair_rows, preferred_element_type=jnp.float32
    ).astype(jnp.bfloat16)
    incoming = lax.all_to_all(
        outgoing.reshape(ep_count, local_experts, capacity, local_width),
        "ep",
        split_axis=0,
        concat_axis=0,
        tiled=True,
    )
    results = expert_apply(incoming, gate_weights, up_weights, down_weights)
    returned = lax.all_to_all(results, "ep", split_axis=0, concat_axis=0, tiled=True)
    weighting = jnp.sum(
        (slot_hot * route_weights.reshape(-1)[:, None]).reshape(tok_count, top_count, -1), axis=1
    )
    combined = jnp.dot(
        weighting,
        returned.reshape(-1, local_width).astype(jnp.float32),
        precision=lax.Precision.HIGHEST,
    )
    out_squares = lax.psum(jnp.sum(combined * combined, axis=1), "tp")
    return (combined * lax.rsqrt(out_squares / D + epsilon)[:, None] * gain_out[None, :]).astype(
        jnp.bfloat16
    )


def solution(mesh):
    placed = (
        P("ep", "tp"),
        P("ep", None),
        P("ep", None),
        P("tp"),
        P("tp"),
        P("ep", "tp", None),
        P("ep", "tp", None),
        P("ep", None, "tp"),
    )
    return jax.shard_map(
        on_device, mesh=mesh, in_specs=placed, out_specs=P("ep", "tp"), check_vma=False
    )
```

profile of v0, /device:TPU:0, one launch (start us, length us, event | category | flops | bytes accessed | tf_op | source)
XLA Modules:
  0.0 181.0 jit_solution(13046292742093290835)
XLA Ops:
  6.5 0.8 copy.27
  7.3 0.1 eq.49
  7.4 0.1 eq.45
  7.5 0.6 reduce-window.6
  8.1 0.2 slice_reduce_fusion
  8.3 0.1 fusion.40
  8.4 1.0 fusion.36
  9.4 11.4 %psum.28 = f32[32]{0:T(128)S(1)} all-reduce(f32[32]{0:T(128)S(1)} %fusion.36), channel_id=1, replica_groups=mesh['ep'=8,'tp'=4] {'tp'}, use_global_device_ids=true, to_apply=%region_5.6 | all-reduce | flops 32 | bytes 256 | tf_op jit(solution)/shard_map/psum | solution.py:38
  20.8 0.9 fusion.38
  21.7 0.6 convolution_convert_fusion
  22.3 31.2 %all_to_all.10 = bf16[8,2,32,1024]{3,2,1,0:T(8,128)(2,1)S(1)} all-to-all(bf16[8,2,32,1024]{3,2,1,0:T(8,128)(2,1)S(1)} %bitcast.56), channel_id=1, replica_groups=mesh['ep'=8,'tp'=4] {'ep'}, dimensions={0} | all-to-all | bytes 2097152 | tf_op jit(solution)/shard_map/all_to_all | solution.py:55
  53.5 4.6 %fusion.23 = bf16[8,2,32,1024]{3,2,0,1:T(8,128)(2,1)} fusion(bf16[2,1024,1024]{2,1,0:T(8,128)(2,1)} %param.14, bf16[8,2,32,1024]{3,2,1,0:T(8,128)(2,1)S(1)} %all_to_all.10), kind=kOutput, calls=%fused_computation.18 | convolution fusion | flops 1074266112 | bytes 6291456 | tf_op jit(solution)/shard_map/secd,edf->secf/dot_general | solution.py:16
  58.1 2.3 %fusion.26 = bf16[8,2,32,1024]{3,2,0,1:T(8,128)(2,1)} fusion(bf16[2,1024,1024]{2,1,0:T(8,128)(2,1)S(1)} %copy-done.2, bf16[8,2,32,1024]{3,2,1,0:T(8,128)(2,1)S(1)} %all_to_all.10), kind=kOutput, calls=%fused_computation.19 | convolution fusion | flops 1074266112 | bytes 6291456 | tf_op jit(solution)/shard_map/secd,edf->secf/dot_general | solution.py:13
  60.4 66.7 %all-reduce.3.cloned.1.call-done = (bf16[8,2,32,1024]{3,2,0,1:T(8,128)(2,1)}, bf16[8,2,32,1024]{3,2,0,1:T(8,128)(2,1)}) async-done(((bf16[8,2,32,1024]{3,2,0,1:T(8,128)(2,1)}, bf16[8,2,32,1024]{3,2,0,1:T(8,128)(2,1)}), (bf16[8,2,32,1024]{3,2,0,1:T(8,128)(2,1)}, bf16[8,2,32,1024]{3,2,0,1:T(8,128)(2,1)})) %all-reduce.3.cloned.1.call-update) | async-done | bytes 2097168 | tf_op jit(solution)/shard_map/psum | solution.py:21
  127.1 4.3 %fusion.20 = bf16[8,2,32,1024]{3,2,0,1:T(8,128)(2,1)S(1)} fusion(bf16[2,1024,1024]{2,1,0:T(8,128)(2,1)} %param.15, bf16[8,2,32,1024]{3,2,0,1:T(8,128)(2,1)} %get-tuple-element.5, bf16[8,2,32,1024]{3,2,0,1:T(8,128)(2,1)} %get-tuple-element.6), kind=kOutput, calls=%fused_computation.17 | convolution fusion | flops 1078460416 | bytes 7340032 | tf_op jit(solution)/shard_map/secf,efd->secd/dot_general | solution.py:24
  131.4 1.1 copy.34
  132.5 4.7 %all-to-all-start.1 = ((bf16[8,2,32,1024]{3,2,1,0:T(8,128)(2,1)}), bf16[8,2,32,1024]{3,2,1,0:T(8,128)(2,1)S(1)}, u32[]{:S(2)}, u32[]{:S(2)}) async-start(bf16[8,2,32,1024]{3,2,1,0:T(8,128)(2,1)} %copy.34), calls=%async_computation.1 | async-start | bytes 2097152 | tf_op jit(solution)/shard_map/all_to_all | solution.py:63
  137.2 0.1 reduce_sum.39
  137.3 0.1 copy.31
  137.4 0.2 select_reduce_fusion
  137.6 26.2 %all-to-all-done.1 = bf16[8,2,32,1024]{3,2,1,0:T(8,128)(2,1)S(1)} async-done(((bf16[8,2,32,1024]{3,2,1,0:T(8,128)(2,1)}), bf16[8,2,32,1024]{3,2,1,0:T(8,128)(2,1)S(1)}, u32[]{:S(2)}, u32[]{:S(2)}) %all-to-all-start.1) | async-done | bytes 1048608 | tf_op jit(solution)/shard_map/all_to_all | solution.py:63
  163.8 0.7 multiply_reduce_fusion
  164.5 8.9 %psum.31 = f32[32]{0:T(128)S(1)} all-reduce(f32[32]{0:T(128)S(1)} %get-tuple-element.7), channel_id=1, replica_groups=mesh['ep'=8,'tp'=4] {'tp'}, use_global_device_ids=true, to_apply=%region_9.10 | all-reduce | flops 32 | bytes 256 | tf_op jit(solution)/shard_map/psum | solution.py:72
  173.4 0.7 multiply_convert_fusion
  (15 shorter events, 0.1 us)
Async XLA Ops:
  6.5 120.5 %all-reduce.3.cloned.1.call-start = ((), (), s32[]{:S(2)}) async-start(), calls=%async_computation.2 | async-start | bytes 4194304 | tf_op jit(solution)/shard_map/psum | solution.py:21
  53.5 4.6 %copy-start.2 = (bf16[2,1024,1024]{2,1,0:T(8,128)(2,1)S(1)}, bf16[2,1024,1024]{2,1,0:T(8,128)(2,1)}, u32[]{:S(2)}) copy-start(bf16[2,1024,1024]{2,1,0:T(8,128)(2,1)} %param.13) | copy-start | bytes 12582916
  131.4 5.9 %copy-start = (f32[32,8]{0,1:T(8,128)S(1)}, f32[32,8]{0,1:T(8,128)}, u32[]{:S(2)}) copy-start(f32[32,8]{0,1:T(8,128)} %param.10) | copy-start | bytes 3076
  132.5 41.0 %copy-start.1 = (f32[1024]{0:T(1024)S(1)}, f32[1024]{0:T(1024)}, u32[]{:S(2)}) copy-start(f32[1024]{0:T(1024)} %param.12) | copy-start | bytes 12292
  132.5 31.3 %all-to-all-start.1 = ((bf16[8,2,32,1024]{3,2,1,0:T(8,128)(2,1)}), bf16[8,2,32,1024]{3,2,1,0:T(8,128)(2,1)S(1)}, u32[]{:S(2)}, u32[]{:S(2)}) async-start(bf16[8,2,32,1024]{3,2,1,0:T(8,128)(2,1)} %copy.34), calls=%async_computation.1 | async-start | bytes 2097152 | tf_op jit(solution)/shard_map/all_to_all | solution.py:63
Sparse Core Ops, SparseCore 0:
  60.5 66.5 all-reduce.2
where the time goes:
time: 181 us
  waiting for transfers between devices  92.9 us (51%)
  blocking collectives  51.6 us (29%)
  between operations  13.5 us (7%)
  matrix products  12.4 us (7%)
  starting transfers between devices  4.74 us (3%)
  other arithmetic  3.59 us (2%)
  local copies, waits for them, and re-layouts  2.39 us (1%)
    psum x1, waiting for transfers between devices, expert_apply(): lax.psum(up_part, 'tp').astype(jnp.float32)  66.7 us
    all_to_all x1, blocking collectives, on_device(): lax.all_to_all(outgoing.reshape(ep_count, local_experts, capacity, local_...  31.2 us
    all_to_all x1, waiting for transfers between devices, on_device(): lax.all_to_all(results, 'ep', split_axis=0, concat_axis=0, tiled=True)  26.2 us
    psum x1, blocking collectives, on_device(): squares = lax.psum(jnp.sum(widened * widened, axis=1), 'tp')  11.4 us
    psum x1, blocking collectives, on_device(): out_squares = lax.psum(jnp.sum(combined * combined, axis=1), 'tp')  8.94 us
    all_to_all x1, starting transfers between devices, on_device(): lax.all_to_all(results, 'ep', split_axis=0, concat_axis=0, tiled=True)  4.74 us
    dot_general x1, matrix products, expert_apply(): jnp.einsum('secd,edf->secf', incoming, up_weights, preferred_element_type...  4.58 us
    dot_general x1, matrix products, expert_apply(): jnp.einsum('secf,efd->secd', hidden, down_weights, preferred_element_type...  4.26 us
  transfers between devices with their start and end apart: 2, of which 2 were waited for; matrix products, arithmetic and copies ran while one was open for 0% of the time, Pallas kernels for 0%

commit v1 on v0

--- a/solution.py
+++ b/solution.py
@@ -1,6 +1,8 @@
 import jax
 import jax.numpy as jnp
 from jax import lax
+from jax.experimental import pallas as pl
+from jax.experimental.pallas import tpu as pltpu
 from jax.sharding import PartitionSpec as P
 
 D = 4096
@@ -75,6 +77,322 @@
     )
 
 
+MESH = pl.DeviceIdType.MESH
+BF16, F32 = jnp.bfloat16, jnp.float32
+
+
+def remote(src, dst, send_sem, recv_sem, target):
+    return pltpu.make_async_remote_copy(
+        src_ref=src,
+        dst_ref=dst,
+        send_sem=send_sem,
+        recv_sem=recv_sem,
+        device_id=target,
+        device_id_type=MESH,
+    )
+
+
+def chip_at(z, k):
+    low = lax.rem(lax.rem(z, 2) + lax.rem(k, 2), 2)
+    high = lax.rem(z // 2 + k // 2, 2)
+    return high * 2 + low
+
+
+def dense_kernel(
+    x_ref, ids_ref, rw_ref, gi_ref, go_ref, gate_hbm, up_hbm, down_hbm, o_ref,
+    w0, w1, dw, xg, xs, ssb, sst, scale, wr, sbuf, r1, s2, r2, keep, hid,
+    acc, dsend, drecv, zsend, zrecv, sq,
+    wsem, ag_s, ag_r, fw_s, fw_r, ss_s, ss_r, p1_s, p1_r, p2_s, p2_r, p3_s, p3_r,
+    p4_s, p4_r, d_s, d_r, z_s, z_r, q_s, q_r,
+):
+    rows, width = x_ref.shape
+    chunks = xg.shape[0]
+    half = w0.shape[3]
+    quarter = half // 2
+    lanes = ssb.shape[2]
+    ep, tp = lax.axis_index("ep"), lax.axis_index("tp")
+    z, c = ep // 2, lax.rem(ep, 2)
+    y, x = tp // 2, lax.rem(tp, 2)
+    xn, yn, dn = y * 2 + 1 - x, (1 - y) * 2 + x, (1 - y) * 2 + 1 - x
+    other = z * 2 + 1 - c
+    first = ((ep, xn), (ep, yn))
+    second = ((ep, yn), (ep, xn))
+    big, small = (x, y), (y, x)
+    planes = ((ep, xn), (ep, yn), (ep, dn))
+
+    mats = (gate_hbm, up_hbm)
+    load0, load1, load2 = [], [], []
+    for e in range(2):
+        for m in range(2):
+            off = pl.multiple_of((1 - big[e]) * half, quarter)
+            load0.append(pltpu.make_async_copy(
+                mats[m].at[e, :, pl.ds(off, half)], w0.at[e, m], wsem.at[e * 2 + m]))
+            for s in range(2):
+                q = small[e] if s else 1 - small[e]
+                off = pl.multiple_of(big[e] * half + q * quarter, quarter)
+                load1.append(pltpu.make_async_copy(
+                    mats[m].at[e, :, pl.ds(off, quarter)], w1.at[e, m, s],
+                    wsem.at[4 + e * 4 + m * 2 + s]))
+        load2.append(pltpu.make_async_copy(down_hbm.at[e], dw.at[e], wsem.at[12 + e]))
+    for load in load0:
+        load.start()
+
+    lane = lax.broadcasted_iota(jnp.int32, (rows, lanes), 1)
+    ids, rw = ids_ref[...], rw_ref[...]
+    route = jnp.zeros((rows, lanes), F32)
+    for k in range(ids.shape[1]):
+        hit = (ids[:, k : k + 1] == lane) | (ids[:, k : k + 1] == lane - lanes // 2)
+        route = route + jnp.where(hit, rw[:, k : k + 1], 0.0)
+    high = route.astype(BF16)
+    low = (route - high.astype(F32)).astype(BF16)
+    xg[0, c, :, :width] = x_ref[...]
+    xg[0, c, :, width:] = jnp.where(
+        lane < lanes // 2, high.astype(F32), low.astype(F32)
+    ).astype(BF16)
+
+    barrier = pltpu.get_barrier_semaphore()
+    greet = [(other, tp)] + [(chip_at(z, k) * 2 + c, tp) for k in range(1, chunks)] + list(planes)
+    for target in greet:
+        pl.semaphore_signal(barrier, inc=1, device_id=target, device_id_type=MESH)
+    pl.semaphore_wait(barrier, len(greet))
+
+    def gather(k):
+        return remote(xg.at[0, c], xg.at[k, c], ag_s.at[k], ag_r.at[k], (chip_at(z, k) * 2 + c, tp))
+
+    def forward(k):
+        return remote(xg.at[k, c], xg.at[k, c], fw_s.at[k], fw_r.at[k], (other, tp))
+
+    forward(0).start()
+    for k in range(1, chunks):
+        gather(k).start()
+    for load in load1 + load2:
+        load.start()
+
+    gain = gi_ref[...]
+    for load in load0:
+        load.wait()
+
+    def phase1(k, e):
+        return remote(sbuf.at[k, e], r1.at[k, e], p1_s.at[k, e], p1_r.at[k, e], first[e])
+
+    def phase2(k, e):
+        return remote(s2.at[k, e], r2.at[k, e], p2_s.at[k, e], p2_r.at[k, e], second[e])
+
+    def phase3(k, e):
+        block = hid.at[k, e, big[e] * 2 + small[e]]
+        return remote(block, block, p3_s.at[k, e], p3_r.at[k, e], second[e])
+
+    def phase4(k, e):
+        block = hid.at[k, e, pl.ds(big[e] * 2, 2)]
+        return remote(block, block, p4_s.at[k, e], p4_r.at[k, e], first[e])
+
+    def across(k):
+        return remote(dsend.at[k], drecv.at[k], d_s.at[k], d_r.at[k], (other, tp))
+
+    def home(k):
+        return remote(zsend.at[k], zrecv.at[k], z_s.at[k], z_r.at[k], (chip_at(z, k) * 2 + c, tp))
+
+    @pl.loop(0, chunks)
+    def _(k):
+        @pl.when(k > 0)
+        def _():
+            gather(k).wait_recv()
+            forward(k).start()
+
+        forward(k).wait_recv()
+        for j in range(2):
+            at = pl.ds(j * rows, rows)
+            xf = xg[k, j, :, :width].astype(F32)
+            ssb[k, at, :] = jnp.broadcast_to(
+                jnp.sum(xf * xf, axis=1, keepdims=True), (rows, lanes))
+            xs[k, at, :] = (xf * gain).astype(BF16)
+            r = xg[k, j, :, width:].astype(F32)
+            for e in range(2):
+                mine = ep * 2 + e
+                hit = (lane == mine) | (lane == mine + lanes // 2)
+                wr[k, e, at, :] = jnp.broadcast_to(
+                    jnp.sum(jnp.where(hit, r, 0.0), axis=1, keepdims=True), (rows, lanes))
+        for e in range(2):
+            for m in range(2):
+                p = jnp.dot(xs[k], w0[e, m], preferred_element_type=F32).astype(BF16)
+                sbuf[k, e, m, 0] = p[:, :quarter]
+                sbuf[k, e, m, 1] = p[:, quarter:]
+            phase1(k, e).start()
+
+    def squares(i):
+        return remote(sst.at[0], sst.at[i], ss_s.at[i], ss_r.at[i], planes[i - 1])
+
+    sst[0] = jnp.transpose(ssb[...].reshape(chunks * 2 * rows, lanes))[:8]
+    for i in range(1, 4):
+        squares(i).start()
+    for load in load1:
+        load.wait()
+
+    def order(i):
+        return lax.rem(i + 1, chunks)
+
+    @pl.loop(0, chunks)
+    def _(i):
+        k = order(i)
+        for e in range(2):
+            phase1(k, e).wait_recv()
+            for m in range(2):
+                p = jnp.dot(xs[k], w1[e, m, 0], preferred_element_type=F32)
+                s2[k, e, m] = (p + r1[k, e, m, 1 - small[e]].astype(F32)).astype(BF16)
+            phase2(k, e).start()
+            for m in range(2):
+                p = jnp.dot(xs[k], w1[e, m, 1], preferred_element_type=F32)
+                keep[k, e, m] = p + r1[k, e, m, small[e]].astype(F32)
+
+    for i in range(1, 4):
+        squares(i).wait_recv()
+    total = jnp.sum(sst[...], axis=0)
+    total = jnp.transpose(jnp.concatenate([total] * (lanes // 8), axis=0))
+    scale[...] = lax.rsqrt(total / D + epsilon).reshape(scale.shape)
+    for load in load2:
+        load.wait()
+
+    @pl.loop(0, chunks + 3)
+    def _(i):
+        @pl.when(i < chunks)
+        def _():
+            k = order(i)
+            s = jnp.concatenate([scale[k]] * (quarter // lanes), axis=1)
+            for e in range(2):
+                phase2(k, e).wait_recv()
+                g = (keep[k, e, 0] + r2[k, e, 0].astype(F32)) * s
+                u = (keep[k, e, 1] + r2[k, e, 1].astype(F32)) * s
+                w = jnp.concatenate([wr[k, e]] * (quarter // lanes), axis=1)
+                h = g / (1.0 + jnp.exp(-g)) * u * w
+                hid[k, e, big[e] * 2 + small[e]] = h.astype(BF16)
+                phase3(k, e).start()
+
+        @pl.when((i >= 1) & (i < chunks + 1))
+        def _():
+            k = order(i - 1)
+            for e in range(2):
+                phase3(k, e).wait_recv()
+                phase4(k, e).start()
+
+        @pl.when((i >= 2) & (i < chunks + 2))
+        def _():
+            k = order(i - 2)
+            for e in range(2):
+                phase4(k, e).wait_recv()
+            hcat = jnp.concatenate([hid[k, e, q] for e in range(2) for q in range(4)], axis=1)
+            for n in range(0, width, half):
+                cols = pl.ds(n, half)
+                down = jnp.concatenate([dw[0, :, cols], dw[1, :, cols]], axis=0)
+                p = jnp.dot(hcat, down, preferred_element_type=F32)
+                acc[k, 0, :, cols] = p[:rows]
+                acc[k, 1, :, cols] = p[rows:]
+            dsend[k] = acc[k, 1 - c].astype(BF16)
+            across(k).start()
+
+        @pl.when((i >= 3) & (i < chunks + 2))
+        def _():
+            k = order(i - 3)
+            across(k).wait_recv()
+            zsend[k] = (acc[k, c] + drecv[k].astype(F32)).astype(BF16)
+            home(k).start()
+
+    def final(i):
+        return remote(sq.at[0], sq.at[i], q_s.at[i], q_r.at[i], planes[i - 1])
+
+    across(0).wait_recv()
+    combined = acc[0, c] + drecv[0].astype(F32)
+    for k in range(1, chunks):
+        home(k).wait_recv()
+        combined = combined + zrecv[k].astype(F32)
+    sq[0] = jnp.broadcast_to(jnp.sum(combined * combined, axis=1, keepdims=True), (rows, lanes))
+    for i in range(1, 4):
+        final(i).start()
+    acc[0, c] = combined
+    for i in range(1, 4):
+        final(i).wait_recv()
+    total = jnp.sum(sq[...], axis=0)
+    out_scale = jnp.concatenate([lax.rsqrt(total / D + epsilon)] * (width // lanes), axis=1)
+    o_ref[...] = (acc[0, c] * out_scale * go_ref[...]).astype(BF16)
+
+    forward(0).wait_send()
+    across(0).wait_send()
+    for i in range(1, 4):
+        gather(i).wait_send()
+        forward(i).wait_send()
+        squares(i).wait_send()
+        across(i).wait_send()
+        home(i).wait_send()
+        final(i).wait_send()
+    for k in range(chunks):
+        for e in range(2):
+            for phase in (phase1, phase2, phase3, phase4):
+                phase(k, e).wait_send()
+
+
+def dense_on_device(
+    tokens, expert_ids, route_weights, gain_in, gain_out, gate_weights, up_weights, down_weights
+):
+    rows, width = tokens.shape
+    ff = gate_weights.shape[2]
+    half, quarter, lanes = ff // 2, ff // 4, 128
+    chunks = lax.axis_size("ep") // 2
+    both = 2 * rows
+    vmem = pl.BlockSpec(memory_space=pltpu.VMEM)
+    hbm = pl.BlockSpec(memory_space=pltpu.HBM)
+    dma = pltpu.SemaphoreType.DMA
+    one, two = dma((chunks,)), dma((chunks, 2))
+    return pl.pallas_call(
+        dense_kernel,
+        out_shape=jax.ShapeDtypeStruct((rows, width), BF16),
+        in_specs=[vmem] * 5 + [hbm] * 3,
+        out_specs=vmem,
+        scratch_shapes=[
+            pltpu.VMEM((2, 2, width, half), BF16),
+            pltpu.VMEM((2, 2, 2, width, quarter), BF16),
+            pltpu.VMEM((2, ff, width), BF16),
+            pltpu.VMEM((chunks, 2, rows, width + lanes), BF16),
+            pltpu.VMEM((chunks, both, width), BF16),
+            pltpu.VMEM((chunks, both, lanes), F32),
+            pltpu.VMEM((4, 8, chunks * both), F32),
+            pltpu.VMEM((chunks, both, lanes), F32),
+            pltpu.VMEM((chunks, 2, both, lanes), F32),
+            pltpu.VMEM((chunks, 2, 2, 2, both, quarter), BF16),
+            pltpu.VMEM((chunks, 2, 2, 2, both, quarter), BF16),
+            pltpu.VMEM((chunks, 2, 2, both, quarter), BF16),
+            pltpu.VMEM((chunks, 2, 2, both, quarter), BF16),
+            pltpu.VMEM((chunks, 2, 2, both, quarter), F32),
+            pltpu.VMEM((chunks, 2, 4, both, quarter), BF16),
+            pltpu.VMEM((chunks, 2, rows, width), F32),
+            pltpu.VMEM((chunks, rows, width), BF16),
+            pltpu.VMEM((chunks, rows, width), BF16),
+            pltpu.VMEM((chunks, rows, width), BF16),
+            pltpu.VMEM((chunks, rows, width), BF16),
+            pltpu.VMEM((4, rows, lanes), F32),
+            dma((14,)),
+        ]
+        + [one] * 6
+        + [two] * 8
+        + [one] * 6,
+        compiler_params=pltpu.CompilerParams(
+            collective_id=0, has_side_effects=True, vmem_limit_bytes=60 * 1024 * 1024
+        ),
+    )(
+        tokens, expert_ids, route_weights, gain_in[None, :], gain_out[None, :],
+        gate_weights, up_weights, down_weights,
+    )
+
+
+def device_program(*args):
+    tokens, expert_ids = args[:2]
+    local_experts = args[5].shape[0]
+    all_experts = local_experts * lax.axis_size("ep")
+    capacity = max(2, 2 * tokens.shape[0] * expert_ids.shape[1] // all_experts)
+    dense = capacity >= tokens.shape[0] and all_experts <= 64
+    if dense and (local_experts, lax.axis_size("ep"), lax.axis_size("tp")) == (2, 8, 4):
+        return dense_on_device(*args)
+    return on_device(*args)
+
+
 def solution(mesh):
     placed = (
         P("ep", "tp"),
@@ -87,5 +405,5 @@
         P("ep", None, "tp"),
     )
     return jax.shard_map(
-        on_device, mesh=mesh, in_specs=placed, out_specs=P("ep", "tp"), check_vma=False
-    )
+        device_program, mesh=mesh, in_specs=placed, out_specs=P("ep", "tp"), check_vma=False
+    )

time: 181 us -> 55.2 us (0.30)
  waiting for transfers between devices: 92.9 us -> 0 us
  blocking collectives: 51.6 us -> 0 us
  Pallas kernels: 0 us -> 50.7 us
  between operations: 13.5 us -> 0.01 us
  matrix products: 12.4 us -> 0 us
  starting transfers between devices: 4.74 us -> 0 us
  other arithmetic: 3.59 us -> 0 us
  local copies, waits for them, and re-layouts: 2.39 us -> 4.2 us
    psum x1 -> x0, waiting for transfers between devices: 66.7 us -> none  [expert_apply(): lax.psum(up_part, 'tp').astype(jnp.float32)]
    pallas_call x0 -> x1, Pallas kernels: none -> 50.7 us  [dense_on_device(): pl.pallas_call(dense_kernel, out_shape=jax.ShapeDtypeStruct((rows, width)...]
    all_to_all x1 -> x0, blocking collectives: 31.2 us -> none  [on_device(): lax.all_to_all(outgoing.reshape(ep_count, local_experts, capacity, local_...]
    all_to_all x1 -> x0, waiting for transfers between devices: 26.2 us -> none  [on_device(): lax.all_to_all(results, 'ep', split_axis=0, concat_axis=0, tiled=True)]
    psum x2 -> x0, blocking collectives: 20.3 us -> none  [the longest x1 11.4 us: on_device(): squares = lax.psum(jnp.sum(widened * widened, axis=1), 'tp')]
    dot_general x5 -> x0, matrix products: 12.4 us -> none  [the longest x1 4.58 us: expert_apply(): jnp.einsum('secd,edf->secf', incoming, up_weights, preferred_element_type...]
    all_to_all x1 -> x0, starting transfers between devices: 4.74 us -> none  [on_device(): lax.all_to_all(results, 'ep', split_axis=0, concat_axis=0, tiled=True)]
    unnamed x8 -> x3, local copies, waits for them, and re-layouts: 0.85 us -> 4.2 us
  transfers between devices with their start and end apart: 2 -> 0, of which waited for: 2 -> 0; matrix products, arithmetic and copies ran while one was open for 0% -> 0% of each run, Pallas kernels for 0% -> 0%
where the time goes in v1:
time: 55.2 us; the launch traced here: 54.9 us
  Pallas kernels  50.7 us (92%)
  local copies, waits for them, and re-layouts  4.2 us (8%)
    pallas_call x1, Pallas kernels, dense_on_device(): pl.pallas_call(dense_kernel, out_shape=jax.ShapeDtypeStruct((rows, width)...  50.7 us
    unnamed x3, local copies, waits for them, and re-layouts  4.2 us

profile of v1, /device:TPU:0, one launch (start us, length us, event | category | flops | bytes accessed | tf_op | source)
XLA Modules:
  0.0 54.9 jit_solution(12517501493647092501)
XLA Ops:
  0.0 1.4 %copy.9.ids_ref = s32[32,8]{1,0:T(8,128)} copy(s32[32,8]{0,1:T(8,128)} %param.9) | data formatting | bytes 2048 | tf_op args[1]
  1.4 1.4 %copy.10.rw_ref = f32[32,8]{1,0:T(8,128)} copy(f32[32,8]{0,1:T(8,128)} %param.10) | data formatting | bytes 2048 | tf_op args[2]
  2.7 50.7 %shard_map.82 = bf16[32,1024]{1,0:T(8,128)(2,1)} custom-call(bf16[32,1024]{1,0:T(8,128)(2,1)} %x_ref.1, s32[32,8]{1,0:T(8,128)} %copy.9.ids_ref, f32[32,8]{1,0:T(8,128)} %copy.10.rw_ref, f32[1,1024]{1,0:T(1,128)} %bitcast.2, f32[1,1024]{1,0:T(1,128)} %bitcast.3, bf16[2,1024,1024]{2,1,0:T(8,128)(2,1)} %gate_hbm.1, bf16[2,1024,1024]{2,1,0:T(8,128)(2,1)} %up_hbm.1, ...), custom_call_target="tpu_custom_call" | custom-call | tf_op jit(solution)/shard_map/pallas_call | solution.py:344
  53.5 1.5 %copy.12 = bf16[32,1024]{1,0:T(8,128)(2,1)} copy(bf16[32,1024]{1,0:T(8,128)(2,1)} %shard_map.82) | data formatting | bytes 131072

commit v2 on v1

--- a/solution.py
+++ b/solution.py
@@ -120,6 +120,11 @@
     big, small = (x, y), (y, x)
     planes = ((ep, xn), (ep, yn), (ep, dn))
 
+    barrier = pltpu.get_barrier_semaphore()
+    greet = [(other, tp)] + [(chip_at(z, k) * 2 + c, tp) for k in range(1, chunks)] + list(planes)
+    for target in greet:
+        pl.semaphore_signal(barrier, inc=1, device_id=target, device_id_type=MESH)
+
     mats = (gate_hbm, up_hbm)
     load0, load1, load2 = [], [], []
     for e in range(2):
@@ -138,11 +143,13 @@
         load.start()
 
     lane = lax.broadcasted_iota(jnp.int32, (rows, lanes), 1)
+    place = lax.broadcasted_iota(jnp.int32, (lanes, rows), 0)
     ids, rw = ids_ref[...], rw_ref[...]
-    route = jnp.zeros((rows, lanes), F32)
-    for k in range(ids.shape[1]):
-        hit = (ids[:, k : k + 1] == lane) | (ids[:, k : k + 1] == lane - lanes // 2)
-        route = route + jnp.where(hit, rw[:, k : k + 1], 0.0)
+    route = jnp.zeros((lanes, rows), F32)
+    for k in range(ids.shape[0]):
+        hit = (ids[k : k + 1] == place) | (ids[k : k + 1] == place - lanes // 2)
+        route = route + jnp.where(hit, rw[k : k + 1], 0.0)
+    route = jnp.transpose(route)
     high = route.astype(BF16)
     low = (route - high.astype(F32)).astype(BF16)
     xg[0, c, :, :width] = x_ref[...]
@@ -150,10 +157,6 @@
         lane < lanes // 2, high.astype(F32), low.astype(F32)
     ).astype(BF16)
 
-    barrier = pltpu.get_barrier_semaphore()
-    greet = [(other, tp)] + [(chip_at(z, k) * 2 + c, tp) for k in range(1, chunks)] + list(planes)
-    for target in greet:
-        pl.semaphore_signal(barrier, inc=1, device_id=target, device_id_type=MESH)
     pl.semaphore_wait(barrier, len(greet))
 
     def gather(k):
@@ -169,8 +172,6 @@
         load.start()
 
     gain = gi_ref[...]
-    for load in load0:
-        load.wait()
 
     def phase1(k, e):
         return remote(sbuf.at[k, e], r1.at[k, e], p1_s.at[k, e], p1_r.at[k, e], first[e])
@@ -213,6 +214,11 @@
                 wr[k, e, at, :] = jnp.broadcast_to(
                     jnp.sum(jnp.where(hit, r, 0.0), axis=1, keepdims=True), (rows, lanes))
         for e in range(2):
+            @pl.when(k == 0)
+            def _():
+                for load in load0[2 * e : 2 * e + 2]:
+                    load.wait()
+
             for m in range(2):
                 p = jnp.dot(xs[k], w0[e, m], preferred_element_type=F32).astype(BF16)
                 sbuf[k, e, m, 0] = p[:, :quarter]
@@ -377,7 +383,7 @@
             collective_id=0, has_side_effects=True, vmem_limit_bytes=60 * 1024 * 1024
         ),
     )(
-        tokens, expert_ids, route_weights, gain_in[None, :], gain_out[None, :],
+        tokens, expert_ids.T, route_weights.T, gain_in[None, :], gain_out[None, :],
         gate_weights, up_weights, down_weights,
     )
 

time: 55.2 us -> 52.4 us (0.949)
  local copies, waits for them, and re-layouts: 4.2 us -> 1.47 us
    unnamed x3 -> x1, local copies, waits for them, and re-layouts: 4.2 us -> 1.47 us
where the time goes in v2:
time: 52.4 us; the launch traced here: 52.2 us
  Pallas kernels  50.8 us (97%)
  local copies, waits for them, and re-layouts  1.47 us (3%)
    pallas_call x1, Pallas kernels, dense_on_device(): pl.pallas_call(dense_kernel, out_shape=jax.ShapeDtypeStruct((rows, width)...  50.8 us
    unnamed x1, local copies, waits for them, and re-layouts  1.47 us

profile of v2, /device:TPU:0, one launch (start us, length us, event | category | flops | bytes accessed | tf_op | source)
XLA Modules:
  0.0 52.2 jit_solution(3621629479895192093)
XLA Ops:
  0.0 50.8 %shard_map.82 = bf16[32,1024]{1,0:T(8,128)(2,1)} custom-call(bf16[32,1024]{1,0:T(8,128)(2,1)} %x_ref.1, s32[8,32]{1,0:T(8,128)} %bitcast.4, f32[8,32]{1,0:T(8,128)} %bitcast.5, f32[1,1024]{1,0:T(1,128)} %bitcast.6, f32[1,1024]{1,0:T(1,128)} %bitcast.7, bf16[2,1024,1024]{2,1,0:T(8,128)(2,1)} %gate_hbm.1, bf16[2,1024,1024]{2,1,0:T(8,128)(2,1)} %up_hbm.1, ...), custom_call_target="tpu_custom_call" | custom-call | tf_op jit(solution)/shard_map/pallas_call | solution.py:350
  50.8 1.5 %copy.10 = bf16[32,1024]{1,0:T(8,128)(2,1)} copy(bf16[32,1024]{1,0:T(8,128)(2,1)} %shard_map.82) | data formatting | bytes 131072

commit v3 on v2

--- a/solution.py
+++ b/solution.py
@@ -100,7 +100,7 @@
 
 def dense_kernel(
     x_ref, ids_ref, rw_ref, gi_ref, go_ref, gate_hbm, up_hbm, down_hbm, o_ref,
-    w0, w1, dw, xg, xs, ssb, sst, scale, wr, sbuf, r1, s2, r2, keep, hid,
+    w0, w1, dw, xg, xs, ssb, sst, scale, wr, sbuf, r1, s2, r2, own, hid,
     acc, dsend, drecv, zsend, zrecv, sq,
     wsem, ag_s, ag_r, fw_s, fw_r, ss_s, ss_r, p1_s, p1_r, p2_s, p2_r, p3_s, p3_r,
     p4_s, p4_r, d_s, d_r, z_s, z_r, q_s, q_r,
@@ -193,6 +193,12 @@
     def home(k):
         return remote(zsend.at[k], zrecv.at[k], z_s.at[k], z_r.at[k], (chip_at(z, k) * 2 + c, tp))
 
+    def own_products(k):
+        for e in range(2):
+            for s in range(2):
+                for m in range(2):
+                    own[k, e, m, s] = jnp.dot(xs[k], w1[e, m, s], preferred_element_type=F32)
+
     @pl.loop(0, chunks)
     def _(k):
         @pl.when(k > 0)
@@ -225,14 +231,22 @@
                 sbuf[k, e, m, 1] = p[:, quarter:]
             phase1(k, e).start()
 
+        @pl.when(k > 0)
+        def _():
+            @pl.when(k == 1)
+            def _():
+                for load in load1:
+                    load.wait()
+
+            own_products(k - 1)
+
     def squares(i):
         return remote(sst.at[0], sst.at[i], ss_s.at[i], ss_r.at[i], planes[i - 1])
 
     sst[0] = jnp.transpose(ssb[...].reshape(chunks * 2 * rows, lanes))[:8]
     for i in range(1, 4):
         squares(i).start()
-    for load in load1:
-        load.wait()
+    own_products(chunks - 1)
 
     def order(i):
         return lax.rem(i + 1, chunks)
@@ -243,73 +257,71 @@
         for e in range(2):
             phase1(k, e).wait_recv()
             for m in range(2):
-                p = jnp.dot(xs[k], w1[e, m, 0], preferred_element_type=F32)
-                s2[k, e, m] = (p + r1[k, e, m, 1 - small[e]].astype(F32)).astype(BF16)
+                away = r1[k, e, m, 1 - small[e]].astype(F32)
+                s2[k, e, m] = (own[k, e, m, 0] + away).astype(BF16)
             phase2(k, e).start()
-            for m in range(2):
-                p = jnp.dot(xs[k], w1[e, m, 1], preferred_element_type=F32)
-                keep[k, e, m] = p + r1[k, e, m, small[e]].astype(F32)
 
     for i in range(1, 4):
         squares(i).wait_recv()
     total = jnp.sum(sst[...], axis=0)
     total = jnp.transpose(jnp.concatenate([total] * (lanes // 8), axis=0))
     scale[...] = lax.rsqrt(total / D + epsilon).reshape(scale.shape)
+
+    @pl.loop(0, chunks)
+    def _(i):
+        k = order(i)
+        s = jnp.concatenate([scale[k]] * (quarter // lanes), axis=1)
+        for e in range(2):
+            w = jnp.concatenate([wr[k, e]] * (quarter // lanes), axis=1)
+            mine = [own[k, e, m, 1] + r1[k, e, m, small[e]].astype(F32) for m in range(2)]
+            phase2(k, e).wait_recv()
+            g = (mine[0] + r2[k, e, 0].astype(F32)) * s
+            u = (mine[1] + r2[k, e, 1].astype(F32)) * s
+            h = g / (1.0 + jnp.exp(-g)) * u * w
+            hid[k, e, big[e] * 2 + small[e]] = h.astype(BF16)
+            phase3(k, e).start()
+
     for load in load2:
         load.wait()
 
-    @pl.loop(0, chunks + 3)
+    @pl.loop(0, chunks)
     def _(i):
-        @pl.when(i < chunks)
+        k = order(i)
+        for e in range(2):
+            phase3(k, e).wait_recv()
+            phase4(k, e).start()
+
+    @pl.loop(0, chunks)
+    def _(i):
+        k = order(i)
+        for e in range(2):
+            phase4(k, e).wait_recv()
+        hcat = jnp.concatenate([hid[k, e, q] for e in range(2) for q in range(4)], axis=1)
+        for n in range(0, width, half):
+            cols = pl.ds(n, half)
+            down = jnp.concatenate([dw[0, :, cols], dw[1, :, cols]], axis=0)
+            p = jnp.dot(hcat, down, preferred_element_type=F32)
+            acc[k, 0, :, cols] = p[:rows]
+            acc[k, 1, :, cols] = p[rows:]
+        dsend[k] = acc[k, 1 - c].astype(BF16)
+        across(k).start()
+
+        @pl.when(i >= 1)
         def _():
-            k = order(i)
-            s = jnp.concatenate([scale[k]] * (quarter // lanes), axis=1)
-            for e in range(2):
-                phase2(k, e).wait_recv()
-                g = (keep[k, e, 0] + r2[k, e, 0].astype(F32)) * s
-                u = (keep[k, e, 1] + r2[k, e, 1].astype(F32)) * s
-                w = jnp.concatenate([wr[k, e]] * (quarter // lanes), axis=1)
-                h = g / (1.0 + jnp.exp(-g)) * u * w
-                hid[k, e, big[e] * 2 + small[e]] = h.astype(BF16)
-                phase3(k, e).start()
-
-        @pl.when((i >= 1) & (i < chunks + 1))
-        def _():
-            k = order(i - 1)
-            for e in range(2):
-                phase3(k, e).wait_recv()
-                phase4(k, e).start()
-
-        @pl.when((i >= 2) & (i < chunks + 2))
-        def _():
-            k = order(i - 2)
-            for e in range(2):
-                phase4(k, e).wait_recv()
-            hcat = jnp.concatenate([hid[k, e, q] for e in range(2) for q in range(4)], axis=1)
-            for n in range(0, width, half):
-                cols = pl.ds(n, half)
-                down = jnp.concatenate([dw[0, :, cols], dw[1, :, cols]], axis=0)
-                p = jnp.dot(hcat, down, preferred_element_type=F32)
-                acc[k, 0, :, cols] = p[:rows]
-                acc[k, 1, :, cols] = p[rows:]
-            dsend[k] = acc[k, 1 - c].astype(BF16)
-            across(k).start()
-
-        @pl.when((i >= 3) & (i < chunks + 2))
-        def _():
-            k = order(i - 3)
-            across(k).wait_recv()
-            zsend[k] = (acc[k, c] + drecv[k].astype(F32)).astype(BF16)
-            home(k).start()
+            b = order(i - 1)
+            across(b).wait_recv()
+            zsend[b] = (acc[b, c] + drecv[b].astype(F32)).astype(BF16)
+            home(b).start()
 
     def final(i):
         return remote(sq.at[0], sq.at[i], q_s.at[i], q_r.at[i], planes[i - 1])
 
-    across(0).wait_recv()
-    combined = acc[0, c] + drecv[0].astype(F32)
+    combined = acc[0, c]
     for k in range(1, chunks):
         home(k).wait_recv()
         combined = combined + zrecv[k].astype(F32)
+    across(0).wait_recv()
+    combined = combined + drecv[0].astype(F32)
     sq[0] = jnp.broadcast_to(jnp.sum(combined * combined, axis=1, keepdims=True), (rows, lanes))
     for i in range(1, 4):
         final(i).start()
@@ -366,7 +378,7 @@
             pltpu.VMEM((chunks, 2, 2, 2, both, quarter), BF16),
             pltpu.VMEM((chunks, 2, 2, both, quarter), BF16),
             pltpu.VMEM((chunks, 2, 2, both, quarter), BF16),
-            pltpu.VMEM((chunks, 2, 2, both, quarter), F32),
+            pltpu.VMEM((chunks, 2, 2, 2, both, quarter), F32),
             pltpu.VMEM((chunks, 2, 4, both, quarter), BF16),
             pltpu.VMEM((chunks, 2, rows, width), F32),
             pltpu.VMEM((chunks, rows, width), BF16),

time: 52.4 us -> 51.2 us (0.977)
  Pallas kernels: 50.8 us -> 49.5 us
    pallas_call x1, Pallas kernels: 50.8 us -> 49.5 us  [dense_on_device(): pl.pallas_call(dense_kernel, out_shape=jax.ShapeDtypeStruct((rows, width)...]
where the time goes in v3:
time: 51.2 us; the launch traced here: 51 us
  Pallas kernels  49.5 us (97%)
  local copies, waits for them, and re-layouts  1.47 us (3%)
    pallas_call x1, Pallas kernels, dense_on_device(): pl.pallas_call(dense_kernel, out_shape=jax.ShapeDtypeStruct((rows, width)...  49.5 us
    unnamed x1, local copies, waits for them, and re-layouts  1.47 us

profile of v3, /device:TPU:0, one launch (start us, length us, event | category | flops | bytes accessed | tf_op | source)
XLA Modules:
  0.0 51.0 jit_solution(10202873578117140072)
XLA Ops:
  0.0 49.5 %shard_map.82 = bf16[32,1024]{1,0:T(8,128)(2,1)} custom-call(bf16[32,1024]{1,0:T(8,128)(2,1)} %x_ref.1, s32[8,32]{1,0:T(8,128)} %bitcast.4, f32[8,32]{1,0:T(8,128)} %bitcast.5, f32[1,1024]{1,0:T(1,128)} %bitcast.6, f32[1,1024]{1,0:T(1,128)} %bitcast.7, bf16[2,1024,1024]{2,1,0:T(8,128)(2,1)} %gate_hbm.1, bf16[2,1024,1024]{2,1,0:T(8,128)(2,1)} %up_hbm.1, ...), custom_call_target="tpu_custom_call" | custom-call | tf_op jit(solution)/shard_map/pallas_call | solution.py:362
  49.5 1.5 %copy.10 = bf16[32,1024]{1,0:T(8,128)(2,1)} copy(bf16[32,1024]{1,0:T(8,128)(2,1)} %shard_map.82) | data formatting | bytes 131072
